TPU v7x, 32 devices: a whole 2x2x4 slice. The times are simulated.
32 devices in a mesh: sp: 8 (over z, x), tp: 4 (over y, core).
Axes of the slice: x: 2, y: 2, z: 4, core: 2. Of those that a mesh axis runs over, the one named last changes fastest.
Arguments:
- mixer_out: bfloat16 [1024, 2048], P('sp'), may hold values from -6 to 6
- out_grad: bfloat16 [1024, 2048], P('sp'), may hold values from -2 to 2
- route_ids: int32 [1024, 2], P('sp'), may hold values from 0 to 7, all different within a row; in each aligned block of 128 rows (0 to 127, 128 to 255, ...) at most 64 rows name the same one
- route_weights: float32 [1024, 2], P('sp'), may hold values from 0.2 to 1.2
- gate_branch: bfloat16 [1024, 2048], P('sp', 'tp'), may hold values from -4 to 4
- states: float32 [1024, 2048], P('sp', 'tp'), may hold values from -6 to 6
- decay: float32 [1024, 2048], P('sp', 'tp'), may hold values from 0 to 1
- w_proj: bfloat16 [2048, 2048], P(None, 'tp'), may hold values from -0.125 to 0.125
- w_gate: bfloat16 [8, 2048, 2048], P('sp', 'tp'), may hold values from -0.125 to 0.125
- w_up: bfloat16 [8, 2048, 2048], P('sp', 'tp'), may hold values from -0.125 to 0.125
- w_down: bfloat16 [8, 2048, 2048], P('sp', 'tp'), may hold values from -0.125 to 0.125
Outputs:
- grad_w_gate: bfloat16 [8, 2048, 2048], P('sp', 'tp')
- grad_w_up: bfloat16 [8, 2048, 2048], P('sp', 'tp')
- grad_w_down: bfloat16 [8, 2048, 2048], P('sp', 'tp')
- grad_w_proj: float32 [2048, 2048], P('sp', 'tp')
- grad_branch: bfloat16 [1024, 2048], P('sp', 'tp')
- grad_drive: float32 [1024, 2048], P('sp', 'tp')
- grad_decay: float32 [1024, 2048], P('sp', 'tp')
Inputs may be any that keep to these rules, and one draw needn't show every extreme that they name: `route_ids`: each row names 2 different experts. In the rows of one index of sp no expert is named more than 64 times, a bound that some block reaches.
All inputs are finite; a program needn't handle non-finite values.
Results may differ from a plain program's by a relative error of at most 0.02.
Values may be sent and summed in bfloat16 or wider, within the bound.
A program may use at most 64 MiB of HBM per device.

v0:
```python
import jax
import jax.numpy as jnp
from jax import lax
from jax.sharding import PartitionSpec as P


def entering(value, axis, join, neutral):
    count, mine = (lax.axis_size(axis), lax.axis_index(axis))
    pieces = jax.tree.map(lambda part: lax.all_gather(part, axis), value)
    pieces = jax.tree.map(lambda part: part[::-1], pieces)
    mine = count - 1 - mine
    so_far = jax.tree.map(
        lambda part, zero: jnp.full_like(part, 0) + jnp.asarray(zero, part.dtype), value, neutral
    )

    def lap(position, so_far):
        longer = join(so_far, jax.tree.map(lambda part: part[position], pieces))
        return jax.tree.map(lambda new, old: jnp.where(position < mine, new, old), longer, so_far)

    return lax.fori_loop(0, count - 1, lap, so_far)


def shifted(block, axis, distance):
    devices = range(lax.axis_size(axis))
    route = [(i - distance, i) for i in devices if i - distance in devices]
    return lax.ppermute(block, axis, route)


def linear_combine(earlier, later):
    return (earlier[0] * later[0], later[0] * earlier[1] + later[1])


def chain_combine(earlier, later):
    return (later[0] * earlier[0], later[1] + later[0] * earlier[1])


def expert_grads(inputs, cotangents, w_gate, w_up, w_down):
    gate_pre = jnp.einsum("esd,efd->esf", inputs, w_gate, preferred_element_type=jnp.float32)
    up_pre = jnp.einsum("esd,efd->esf", inputs, w_up, preferred_element_type=jnp.float32)
    sigmoid_gate = jax.nn.sigmoid(gate_pre)
    silu_gate = gate_pre * sigmoid_gate
    hidden = (silu_gate * up_pre).astype(jnp.bfloat16)
    hidden_grad = jnp.einsum("esd,efd->esf", cotangents, w_down, preferred_element_type=jnp.float32)
    up_grad = (hidden_grad * silu_gate).astype(jnp.bfloat16)
    gate_grad = (
        hidden_grad * up_pre * sigmoid_gate * (1.0 + gate_pre * (1.0 - sigmoid_gate))
    ).astype(jnp.bfloat16)
    grad_gate = jnp.einsum(
        "esf,esd->efd", gate_grad, inputs, preferred_element_type=jnp.float32
    ).astype(jnp.bfloat16)
    grad_up = jnp.einsum(
        "esf,esd->efd", up_grad, inputs, preferred_element_type=jnp.float32
    ).astype(jnp.bfloat16)
    grad_down = jnp.einsum(
        "esf,esd->efd", hidden, cotangents, preferred_element_type=jnp.float32
    ).astype(jnp.bfloat16)
    partial_value = jnp.einsum(
        "esf,efd->esd", gate_grad, w_gate, preferred_element_type=jnp.float32
    )
    partial_value = partial_value + jnp.einsum(
        "esf,efd->esd", up_grad, w_up, preferred_element_type=jnp.float32
    )
    return (grad_gate, grad_up, grad_down, partial_value.astype(jnp.bfloat16))


def local(
    mixer_out,
    out_grad,
    route_ids,
    route_weights,
    gate_branch,
    states,
    decay,
    w_proj,
    w_gate,
    w_up,
    w_down,
):
    tok_rows, model_width = mixer_out.shape
    top_count = route_ids.shape[1]
    local_experts = w_gate.shape[0]
    sp_size = lax.axis_size("sp")
    tp_size = lax.axis_size("tp")
    experts = local_experts * sp_size
    capacity = 2 * top_count * tok_rows // experts
    routes = tok_rows * top_count
    flat_ids = route_ids.reshape(-1)
    onehot = (flat_ids[:, None] == jnp.arange(experts, dtype=jnp.int32)[None, :]).astype(jnp.int32)
    position = jnp.sum(jnp.cumsum(onehot, axis=0) * onehot, axis=1) - 1
    bucket = flat_ids % local_experts * sp_size + flat_ids // local_experts
    slot_index = bucket * capacity + position
    source = (
        jnp.full((experts * capacity,), routes, jnp.int32)
        .at[slot_index]
        .set(jnp.arange(routes, dtype=jnp.int32))
    )
    scaled = (route_weights[:, :, None] * out_grad[:, None, :].astype(jnp.float32)).astype(
        jnp.bfloat16
    )
    scaled_pad = jnp.concatenate(
        [scaled.reshape(routes, model_width), jnp.zeros((1, model_width), jnp.bfloat16)], axis=0
    )
    token_pad = jnp.concatenate([mixer_out, jnp.zeros((1, model_width), jnp.bfloat16)], axis=0)
    slot_shape = (local_experts, sp_size, capacity, model_width)
    x_send = token_pad[source // top_count].reshape(slot_shape)
    c_send = scaled_pad[source].reshape(slot_shape)
    slot_share = capacity // tp_size
    first_slot = lax.axis_index("tp") * slot_share
    x_part = lax.dynamic_slice_in_dim(x_send, first_slot, slot_share, 2)
    c_part = lax.dynamic_slice_in_dim(c_send, first_slot, slot_share, 2)
    x_part, c_part = (
        lax.all_to_all(x_part, "sp", split_axis=1, concat_axis=1, tiled=True),
        lax.all_to_all(c_part, "sp", split_axis=1, concat_axis=1, tiled=True),
    )
    x_recv, c_recv = (
        lax.all_gather(x_part, "tp", axis=2, tiled=True),
        lax.all_gather(c_part, "tp", axis=2, tiled=True),
    )
    grad_gate, grad_up, grad_down, partial_value = expert_grads(
        x_recv.reshape(local_experts, -1, model_width),
        c_recv.reshape(local_experts, -1, model_width),
        w_gate,
        w_up,
        w_down,
    )
    pieces = lax.all_to_all(
        partial_value.reshape(slot_shape), "tp", split_axis=2, concat_axis=0, tiled=True
    )
    summed = jnp.sum(
        pieces.reshape(tp_size, local_experts, sp_size, slot_share, model_width).astype(
            jnp.float32
        ),
        axis=0,
    )
    returned = lax.all_to_all(
        summed.astype(jnp.bfloat16), "sp", split_axis=1, concat_axis=1, tiled=True
    ).astype(summed.dtype)
    offset = position - first_slot
    inside = ((offset >= 0) & (offset < slot_share)).astype(jnp.float32)
    index_part = bucket * slot_share + jnp.clip(offset, 0, slot_share - 1)
    picked = returned.reshape(-1, model_width)[index_part] * inside[:, None]
    token_part = jnp.sum(picked.reshape(tok_rows, top_count, model_width), axis=1)
    routed_total = lax.psum(token_part.astype(jnp.bfloat16), "tp").astype(jnp.float32)
    mid_grad = (out_grad.astype(jnp.float32) + routed_total).astype(jnp.bfloat16)
    gated = (gate_branch.astype(jnp.float32) * states).astype(jnp.bfloat16)
    proj_grad = lax.psum_scatter(
        lax.dot_general(
            mid_grad, gated, (((0,), (0,)), ((), ())), preferred_element_type=jnp.float32
        ).astype(jnp.bfloat16),
        "sp",
        scatter_dimension=0,
        tiled=True,
    ).astype(jnp.float32)
    act_grad = jnp.dot(mid_grad, w_proj, preferred_element_type=jnp.float32)
    branch_grad = (act_grad * states).astype(jnp.bfloat16)
    state_grad = act_grad * gate_branch.astype(jnp.float32)
    channels = decay.shape[1]
    next_decay = jnp.concatenate([decay[1:], jnp.ones((1, channels), jnp.float32)], axis=0)
    decay_prod, local_grad = lax.associative_scan(
        linear_combine, (next_decay[::-1], state_grad[::-1]), axis=0
    )
    decay_prod = decay_prod[::-1]
    local_grad = local_grad[::-1]
    head_decay = decay[0]
    carried = entering(
        (head_decay * decay_prod[0], head_decay * local_grad[0]),
        "sp",
        chain_combine,
        (jnp.ones_like(head_decay), jnp.zeros_like(head_decay)),
    )
    drive_grad = local_grad + decay_prod * carried[1][None, :]
    before = shifted(states[-1:], "sp", 1)
    previous = jnp.concatenate([before, states[:-1]], axis=0)
    decay_grad = drive_grad * previous
    return (grad_gate, grad_up, grad_down, proj_grad, branch_grad, drive_grad, decay_grad)


def solution(mesh):
    placed = (
        P("sp", None),
        P("sp", None),
        P("sp", None),
        P("sp", None),
        P("sp", "tp"),
        P("sp", "tp"),
        P("sp", "tp"),
        P(None, "tp"),
        P("sp", "tp", None),
        P("sp", "tp", None),
        P("sp", "tp", None),
    )
    return jax.shard_map(
        local,
        mesh=mesh,
        in_specs=placed,
        out_specs=(
            P("sp", "tp", None),
            P("sp", "tp", None),
            P("sp", "tp", None),
            P("sp", "tp"),
            P("sp", "tp"),
            P("sp", "tp"),
            P("sp", "tp"),
        ),
        check_vma=False,
    )
```

profile of v0, /device:TPU:0, one launch (start us, length us, event | category | flops | bytes accessed | tf_op | source)
XLA Modules:
  0.0 276.9 jit_solution(13569955936952840303)
XLA Ops:
  13.2 3.3 %gather_fusion.1 = bf16[512,2048]{1,0:T(8,128)(2,1)} fusion(bf16[129,2048]{1,0:T(8,128)(2,1)S(1)} %concatenate.49, s32[1024]{0:T(1024)S(1)} %get-tuple-element.176), kind=kCustom, calls=%fused_computation.1 | custom fusion | bytes 4196352 | tf_op jit(solution)/shard_map/gather | solution.py:105
  17.6 21.7 %all_to_all.27 = bf16[1,8,16,2048]{3,2,0,1:T(8,128)(2,1)} all-to-all(bf16[1,8,16,2048]{3,2,0,1:T(8,128)(2,1)S(1)} %constant_dynamic-slice_fusion.2), channel_id=1, replica_groups=mesh['sp'=8,'tp'=4] {'sp'}, dimensions={1} | all-to-all | bytes 1048576 | tf_op jit(solution)/shard_map/all_to_all | solution.py:112
  39.4 2.4 mul.210
  41.8 3.7 %mul.211 = f32[256,2048]{1,0:T(8,128)} reshape(f32[128,2,2048]{2,1,0:T(2,128)} %mul.210) | data formatting | bytes 4194304 | tf_op jit(solution)/shard_map/mul | solution.py:97
  45.7 2.1 multiply_convert_fusion
  47.9 3.3 %gather_fusion = bf16[512,2048]{1,0:T(8,128)(2,1)} fusion(bf16[257,2048]{1,0:T(8,128)(2,1)S(1)} %concatenate.48, s32[1024]{0:T(1024)S(1)} %get-tuple-element.177), kind=kCustom, calls=%fused_computation | custom fusion | bytes 4196352 | tf_op jit(solution)/shard_map/gather | solution.py:106
  52.2 17.3 %all_to_all.28 = bf16[1,8,16,2048]{3,2,0,1:T(8,128)(2,1)} all-to-all(bf16[1,8,16,2048]{3,2,0,1:T(8,128)(2,1)S(1)} %constant_dynamic-slice_fusion.3), channel_id=1, replica_groups=mesh['sp'=8,'tp'=4] {'sp'}, dimensions={1} | all-to-all | bytes 1048576 | tf_op jit(solution)/shard_map/all_to_all | solution.py:113
  69.7 3.0 %fusion.5 = f32[512,512]{1,0:T(8,128)S(1)} fusion(bf16[512,2048]{1,0:T(8,128)(2,1)} %bitcast.85, bf16[1,512,2048]{2,1,0:T(8,128)(2,1)S(1)} %copy-done), kind=kOutput, calls=%fused_computation.17 | convolution fusion | flops 1073741824 | bytes 5242880 | tf_op jit(solution)/shard_map/esd,efd->esf/dot_general | solution.py:38
  72.7 2.2 fusion.8
  75.0 16.4 %all-gather.5.cloned.1.call-done = bf16[1,8,64,2048]{3,2,0,1:T(8,128)(2,1)} async-done(((bf16[1,8,16,2048]{3,2,0,1:T(8,128)(2,1)}), bf16[1,8,64,2048]{3,2,0,1:T(8,128)(2,1)}) %all-gather.5.cloned.1.call-update) | async-done | bytes 2097168 | tf_op jit(solution)/shard_map/all_gather | solution.py:117
  91.4 4.0 %multiply_convert_fusion.2 = (bf16[512,512]{1,0:T(8,128)(2,1)S(1)}, bf16[512,512]{1,0:T(8,128)(2,1)S(1)}) fusion(f32[512,512]{1,0:T(8,128)S(1)} %fusion.5, f32[512,512]{1,0:T(8,128)} %fusion.8, bf16[512,2048]{1,0:T(8,128)(2,1)} %bitcast.89, bf16[1,512,2048]{2,1,0:T(8,128)(2,1)} %param.23), kind=kOutput, calls=%fused_computation.28 | convolution fusion | flops 1077149696 | bytes 7340032 | tf_op jit(solution)/shard_map/esd,efd->esf/dot_general | solution.py:43
  98.7 2.5 copy.37
  101.2 3.7 %all-to-all-start.2 = ((bf16[1,8,64,2048]{3,1,0,2:T(8,128)(2,1)}), bf16[1,8,64,2048]{3,1,0,2:T(8,128)(2,1)S(1)}, u32[]{:S(2)}, u32[]{:S(2)}) async-start(bf16[1,8,64,2048]{3,1,0,2:T(8,128)(2,1)} %copy.37), calls=%async_computation.2 | async-start | bytes 4194304 | tf_op jit(solution)/shard_map/all_to_all | solution.py:126
  105.5 3.4 %collective-permute-start = (f32[1,512]{1,0:T(1,128)}, f32[1,512]{1,0:T(1,128)S(1)}, u32[]{:S(2)}, u32[]{:S(2)}) collective-permute-start(f32[1,512]{1,0:T(1,128)} %slice.319), channel_id=1, source_target_pairs={{0,4},{4,8},{8,12},{12,16},{16,20},{20,24},{24,28},{1,5},{5,9},{9,... | collective-permute-start | bytes 6152 | tf_op jit(solution)/shard_map/ppermute | solution.py:26
  108.9 21.7 %all-to-all-done.2 = bf16[1,8,64,2048]{3,1,0,2:T(8,128)(2,1)S(1)} async-done(((bf16[1,8,64,2048]{3,1,0,2:T(8,128)(2,1)}), bf16[1,8,64,2048]{3,1,0,2:T(8,128)(2,1)S(1)}, u32[]{:S(2)}, u32[]{:S(2)}) %all-to-all-start.2) | async-done | bytes 2097184 | tf_op jit(solution)/shard_map/all_to_all | solution.py:126
  132.1 5.6 %all-to-all-start.3 = ((bf16[1,8,16,2048]{3,2,0,1:T(8,128)(2,1)}), bf16[1,8,16,2048]{3,2,0,1:T(8,128)(2,1)S(1)}, u32[]{:S(2)}, u32[]{:S(2)}) async-start(bf16[1,8,16,2048]{3,2,0,1:T(8,128)(2,1)} %copy.38), calls=%async_computation.3 | async-start | bytes 1048576 | tf_op jit(solution)/shard_map/all_to_all | solution.py:135
  141.9 4.3 %fusion = bf16[1,512,2048]{2,1,0:T(8,128)(2,1)} fusion(bf16[512,512]{1,0:T(8,128)(2,1)S(1)} %copy-done.14, bf16[512,2048]{1,0:T(8,128)(2,1)} %bitcast.86), kind=kOutput, calls=%fused_computation.12 | convolution fusion | flops 1074790400 | bytes 4718592 | tf_op jit(solution)/shard_map/esf,esd->efd/dot_general | solution.py:48
  146.3 2.7 fusion.2
  149.0 3.0 %all-to-all-done.3 = bf16[1,8,16,2048]{3,2,0,1:T(8,128)(2,1)S(1)} async-done(((bf16[1,8,16,2048]{3,2,0,1:T(8,128)(2,1)}), bf16[1,8,16,2048]{3,2,0,1:T(8,128)(2,1)S(1)}, u32[]{:S(2)}, u32[]{:S(2)}) %all-to-all-start.3) | async-done | bytes 524320 | tf_op jit(solution)/shard_map/all_to_all | solution.py:135
  152.1 1.5 gather_fusion.2
  153.6 2.2 gather.14
  155.8 5.6 %multiply_reduce_fusion = bf16[128,2048]{1,0:T(8,128)(2,1)} fusion(f32[128,2,2048]{2,1,0:T(2,128)} %gather.14, f32[128,2]{1,0:T(8,128)S(1)} %copy-done.16), kind=kLoop, calls=%fused_computation.24 | loop fusion | flops 786432 | bytes 2622464 | tf_op jit(solution)/shard_map/reduce_sum | solution.py:142
  161.6 4.2 %fusion.1 = bf16[1,512,2048]{2,1,0:T(8,128)(2,1)} fusion(bf16[512,512]{1,0:T(8,128)(2,1)S(1)} %copy-done.9, bf16[512,2048]{1,0:T(8,128)(2,1)} %bitcast.87), kind=kOutput, calls=%fused_computation.13 | convolution fusion | flops 1074790400 | bytes 4718592 | tf_op jit(solution)/shard_map/esf,esd->efd/dot_general | solution.py:51
  165.8 27.5 %all-reduce.34.cloned.1.call-done = bf16[128,2048]{1,0:T(8,128)(2,1)} async-done(((bf16[128,2048]{1,0:T(8,128)(2,1)}), bf16[128,2048]{1,0:T(8,128)(2,1)}) %all-reduce.34.cloned.1.call-update) | async-done | bytes 524304 | tf_op jit(solution)/shard_map/psum | solution.py:143
  193.3 2.9 %convert_multiply_fusion = (f32[128,512]{1,0:T(8,128)S(1)}, bf16[128,512]{1,0:T(8,128)(2,1)}) fusion(bf16[128,512]{1,0:T(8,128)(2,1)S(1)} %copy-done.10, f32[128,512]{1,0:T(8,128)S(1)} %copy-done.4, bf16[2048,512]{1,0:T(8,128)(2,1)} %param.20, bf16[128,2048]{1,0:T(8,128)(2,1)} %all-reduce.34.cloned.1.call-done, bf16[128,2048]{1,0:T(8,128)(2,1)S(1)} %copy-done.3), kind=kOutput, calls=%fused_computation.33 | convolution fusion | flops 269746176 | bytes 3932160 | tf_op jit(solution)/shard_map/dot_general | solution.py:154
  197.5 2.1 convolution_convert_fusion
  202.2 26.2 %all-gather = f32[8,1,512]{2,1,0:T(1,128)S(1)} all-gather(f32[1,1,512]{2,1,0:T(1,128)S(1)} %get-tuple-element.137), channel_id=1, replica_groups=mesh['sp'=8,'tp'=4] {'sp'}, dimensions={0}, use_global_device_ids=true | all-gather | bytes 18432 | tf_op jit(solution)/shard_map/all_gather | solution.py:9
  228.5 26.1 %all-gather.1 = f32[8,1,512]{2,1,0:T(1,128)S(1)} all-gather(f32[1,1,512]{2,1,0:T(1,128)S(1)} %get-tuple-element.136), channel_id=1, replica_groups=mesh['sp'=8,'tp'=4] {'sp'}, dimensions={0}, use_global_device_ids=true | all-gather | bytes 18432 | tf_op jit(solution)/shard_map/all_gather | solution.py:9
  256.6 1.7 rev.14
  258.3 1.7 rev.15
  260.9 7.6 %reduce-scatter.2.cloned.1.call-done = bf16[256,512]{1,0:T(8,128)(2,1)} async-done(((bf16[2048,512]{1,0:T(8,128)(2,1)}), bf16[256,512]{1,0:T(8,128)(2,1)}) %reduce-scatter.2.cloned.1.call-update) | async-done | bytes 262160 | tf_op jit(solution)/shard_map/reduce_scatter | solution.py:146
  268.5 1.8 convert_element_type.103
  (227 shorter events, 24.5 us)
Async XLA Ops:
  7.2 62.5 %copy-start = (bf16[1,512,2048]{2,1,0:T(8,128)(2,1)S(1)}, bf16[1,512,2048]{2,1,0:T(8,128)(2,1)}, u32[]{:S(2)}) copy-start(bf16[1,512,2048]{2,1,0:T(8,128)(2,1)} %param.21) | copy-start | bytes 6291460
  7.2 62.4 %all-gather.7.cloned.1.call-start = ((), (), s32[]{:S(2)}) async-start(), calls=%async_computation.6 | async-start | bytes 2621440 | tf_op jit(solution)/shard_map/all_gather | solution.py:116
  16.4 22.9 %copy-start.2 = (bf16[128,2048]{1,0:T(8,128)(2,1)S(1)}, bf16[128,2048]{1,0:T(8,128)(2,1)}, u32[]{:S(2)}) copy-start(bf16[128,2048]{1,0:T(8,128)(2,1)} %param.14) | copy-start | bytes 1572868
  39.3 52.1 %all-gather.5.cloned.1.call-start = ((), (), s32[]{:S(2)}) async-start(), calls=%async_computation.5 | async-start | bytes 2621440 | tf_op jit(solution)/shard_map/all_gather | solution.py:117
  41.7 3.7 %copy-start.17 = (f32[128,2]{0,1:T(2,128)S(1)}, f32[128,2]{0,1:T(2,128)}, u32[]{:S(2)}) copy-start(f32[128,2]{0,1:T(2,128)} %param.16) | copy-start | bytes 3076
  69.6 3.1 %copy-start.6 = (bf16[1,512,2048]{2,1,0:T(8,128)(2,1)S(1)}, bf16[1,512,2048]{2,1,0:T(8,128)(2,1)}, u32[]{:S(2)}) copy-start(bf16[1,512,2048]{2,1,0:T(8,128)(2,1)} %param.22) | copy-start | bytes 6291460
  69.6 3.0 %copy-start.18 = (bf16[1,8,64,2048]{3,2,0,1:T(8,128)(2,1)S(1)}, bf16[1,8,64,2048]{3,2,0,1:T(8,128)(2,1)}, u32[]{:S(2)}) copy-start(bf16[1,8,64,2048]{3,2,0,1:T(8,128)(2,1)} %all-gather.7.cloned.1.call-done) | copy-start | bytes 6291460
  72.7 18.7 %copy-start.20 = (f32[512,512]{1,0:T(8,128)}, f32[512,512]{1,0:T(8,128)S(1)}, u32[]{:S(2)}) copy-start(f32[512,512]{1,0:T(8,128)S(1)} %fusion.5) | copy-start | bytes 3145732
  95.4 1.3 copy-start.13
  95.5 1.3 copy-start.8
  95.5 2.0 copy-start.7
  101.2 3.8 %copy-start.4 = (f32[128,512]{1,0:T(8,128)S(1)}, f32[128,512]{1,0:T(8,128)}, u32[]{:S(2)}) copy-start(f32[128,512]{1,0:T(8,128)} %param.18) | copy-start | bytes 786436
  101.2 29.4 %all-to-all-start.2 = ((bf16[1,8,64,2048]{3,1,0,2:T(8,128)(2,1)}), bf16[1,8,64,2048]{3,1,0,2:T(8,128)(2,1)S(1)}, u32[]{:S(2)}, u32[]{:S(2)}) async-start(bf16[1,8,64,2048]{3,1,0,2:T(8,128)(2,1)} %copy.37), calls=%async_computation.2 | async-start | bytes 4194304 | tf_op jit(solution)/shard_map/all_to_all | solution.py:126
  105.5 154.5 %collective-permute-start = (f32[1,512]{1,0:T(1,128)}, f32[1,512]{1,0:T(1,128)S(1)}, u32[]{:S(2)}, u32[]{:S(2)}) collective-permute-start(f32[1,512]{1,0:T(1,128)} %slice.319), channel_id=1, source_target_pairs={{0,4},{4,8},{8,12},{12,16},{16,20},{20,24},{24,28},{1,5},{5,9},{9,... | collective-permute-start | bytes 6152 | tf_op jit(solution)/shard_map/ppermute | solution.py:26
  130.6 7.5 %copy-start.15 = (f32[128,512]{1,0:T(8,128)S(1)}, f32[128,512]{1,0:T(8,128)}, u32[]{:S(2)}) copy-start(f32[128,512]{1,0:T(8,128)} %param.19) | copy-start | bytes 786436
  132.1 9.8 %copy-start.14 = (bf16[512,512]{1,0:T(8,128)(2,1)S(1)}, bf16[512,512]{1,0:T(8,128)(2,1)}, u32[]{:S(2)}) copy-start(bf16[512,512]{1,0:T(8,128)(2,1)} %copy-done.13) | copy-start | bytes 1572868
  132.1 19.9 %all-to-all-start.3 = ((bf16[1,8,16,2048]{3,2,0,1:T(8,128)(2,1)}), bf16[1,8,16,2048]{3,2,0,1:T(8,128)(2,1)S(1)}, u32[]{:S(2)}, u32[]{:S(2)}) async-start(bf16[1,8,16,2048]{3,2,0,1:T(8,128)(2,1)} %copy.38), calls=%async_computation.3 | async-start | bytes 1048576 | tf_op jit(solution)/shard_map/all_to_all | solution.py:135
  137.7 55.6 %all-reduce.34.cloned.1.call-start = ((), (), s32[]{:S(2)}) async-start(), calls=%async_computation.7 | async-start | bytes 1048576 | tf_op jit(solution)/shard_map/psum | solution.py:143
  141.9 4.4 %copy-start.19 = (bf16[1,8,64,2048]{3,2,0,1:T(8,128)(2,1)S(1)}, bf16[1,8,64,2048]{3,2,0,1:T(8,128)(2,1)}, u32[]{:S(2)}) copy-start(bf16[1,8,64,2048]{3,2,0,1:T(8,128)(2,1)} %all-gather.5.cloned.1.call-done) | copy-start | bytes 6291460
  141.9 4.4 %copy-start.21 = (f32[512,512]{1,0:T(8,128)S(1)}, f32[512,512]{1,0:T(8,128)}, u32[]{:S(2)}) copy-start(f32[512,512]{1,0:T(8,128)} %copy-done.20) | copy-start | bytes 3145732
  141.9 4.4 %copy-start.22 = (f32[512,512]{1,0:T(8,128)S(1)}, f32[512,512]{1,0:T(8,128)}, u32[]{:S(2)}) copy-start(f32[512,512]{1,0:T(8,128)} %fusion.8) | copy-start | bytes 3145732
  153.6 2.3 copy-start.16
  155.8 5.7 %copy-start.9 = (bf16[512,512]{1,0:T(8,128)(2,1)S(1)}, bf16[512,512]{1,0:T(8,128)(2,1)}, u32[]{:S(2)}) copy-start(bf16[512,512]{1,0:T(8,128)(2,1)} %copy-done.8) | copy-start | bytes 1572868
  161.5 31.8 %copy-start.3 = (bf16[128,2048]{1,0:T(8,128)(2,1)S(1)}, bf16[128,2048]{1,0:T(8,128)(2,1)}, u32[]{:S(2)}) copy-start(bf16[128,2048]{1,0:T(8,128)(2,1)} %param.14) | copy-start | bytes 1572868
  161.5 31.8 %copy-start.10 = (bf16[128,512]{1,0:T(8,128)(2,1)S(1)}, bf16[128,512]{1,0:T(8,128)(2,1)}, u32[]{:S(2)}) copy-start(bf16[128,512]{1,0:T(8,128)(2,1)} %param.17) | copy-start | bytes 393220
  161.5 107.0 %reduce-scatter.2.cloned.1.call-start = ((), (), s32[]{:S(2)}) async-start(), calls=%async_computation.8 | async-start | bytes 2359296 | tf_op jit(solution)/shard_map/reduce_scatter | solution.py:146
  165.8 30.9 %copy-start.11 = (f32[64,512]{1,0:T(8,128)S(1)}, f32[64,512]{1,0:T(8,128)}, u32[]{:S(2)}) copy-start(f32[64,512]{1,0:T(8,128)} %slice.251) | copy-start | bytes 393220
  196.2 1.3 copy-start.5
  200.2 0.9 copy-start.12
  255.1 15.2 %copy-start.1 = (bf16[1,512,2048]{2,1,0:T(8,128)(2,1)S(1)}, bf16[1,512,2048]{2,1,0:T(8,128)(2,1)}, u32[]{:S(2)}) copy-start(bf16[1,512,2048]{2,1,0:T(8,128)(2,1)} %param.21) | copy-start | bytes 6291460
Sparse Core Ops, SparseCore 0:
  39.4 21.5 all-gather.6
  69.7 21.6 all-gather.4
  161.6 31.6 all-reduce.33
  199.7 68.7 reduce-scatter.1
where the time goes:
time: 278 us; the launch traced here: 277 us
  blocking collectives  91.4 us (33%)
  waiting for transfers between devices  76.3 us (27%)
  local copies, waits for them, and re-layouts  37.5 us (13%)
  matrix products  28.1 us (10%)
  other arithmetic  15.3 us (6%)
  between operations  14.8 us (5%)
  starting transfers between devices  13.1 us (5%)
    all_gather x2, blocking collectives, entering(): pieces = jax.tree.map(lambda part: lax.all_gather(part, axis), value)  52.4 us
    psum x1, waiting for transfers between devices, local(): lax.psum(token_part.astype(jnp.bfloat16), 'tp').astype(jnp.float32)  27.5 us
    all_to_all x1, blocking collectives, local(): lax.all_to_all(x_part, 'sp', split_axis=1, concat_axis=1, tiled=True)  21.7 us
    all_to_all x1, waiting for transfers between devices, local(): lax.all_to_all(partial_value.reshape(slot_shape), 'tp', split_axis=2, con...  21.7 us
    all_to_all x1, blocking collectives, local(): lax.all_to_all(c_part, 'sp', split_axis=1, concat_axis=1, tiled=True)  17.3 us
    all_gather x1, waiting for transfers between devices, local(): lax.all_gather(c_part, 'tp', axis=2, tiled=True)  16.4 us
    reduce_scatter x1, waiting for transfers between devices, local(): lax.psum_scatter(lax.dot_general(mid_grad, gated, (((0,), (0,)), ((), ())...  7.59 us
    mul x3, local copies, waits for them, and re-layouts, local(): route_weights[:, :, None] * out_grad[:, None, :].astype(jnp.float32)  6.17 us
  transfers between devices with their start and end apart: 7, of which 5 were waited for; matrix products, arithmetic and copies ran while one was open for 21% of the time, Pallas kernels for 0%

commit v1 on v0

--- a/solution.py
+++ b/solution.py
@@ -140,7 +140,9 @@
     index_part = bucket * slot_share + jnp.clip(offset, 0, slot_share - 1)
     picked = returned.reshape(-1, model_width)[index_part] * inside[:, None]
     token_part = jnp.sum(picked.reshape(tok_rows, top_count, model_width), axis=1)
-    routed_total = lax.psum(token_part.astype(jnp.bfloat16), "tp").astype(jnp.float32)
+    routed_total = (
+        lax.all_gather(token_part.astype(jnp.bfloat16), "tp").sum(axis=0).astype(jnp.float32)
+    )
     mid_grad = (out_grad.astype(jnp.float32) + routed_total).astype(jnp.bfloat16)
     gated = (gate_branch.astype(jnp.float32) * states).astype(jnp.bfloat16)
     proj_grad = lax.psum_scatter(

time: 278 us -> 266 us (0.957)
  waiting for transfers between devices: 76.3 us -> 44.1 us
  blocking collectives: 91.4 us -> 120 us
  local copies, waits for them, and re-layouts: 37.5 us -> 32.4 us
  starting transfers between devices: 13.1 us -> 9.61 us
    all_to_all x0 -> x1, blocking collectives: none -> 28.1 us  [local(): lax.all_to_all(partial_value.reshape(slot_shape), 'tp', split_axis=2, con...]
    psum x1 -> x0, waiting for transfers between devices: 27.5 us -> none  [local(): lax.psum(token_part.astype(jnp.bfloat16), 'tp').astype(jnp.float32)]
    all_to_all x1 -> x0, waiting for transfers between devices: 21.7 us -> none  [local(): lax.all_to_all(partial_value.reshape(slot_shape), 'tp', split_axis=2, con...]
    all_to_all x1, waiting for transfers between devices: 3.01 us -> 13.7 us  [local(): lax.all_to_all(summed.astype(jnp.bfloat16), 'sp', split_axis=1, concat_ax...]
    all_gather x0 -> x1, waiting for transfers between devices: none -> 6.58 us  [local(): lax.all_gather(token_part.astype(jnp.bfloat16), 'tp').sum(axis=0)]
    all_to_all x1 -> x0, starting transfers between devices: 3.74 us -> none  [local(): lax.all_to_all(partial_value.reshape(slot_shape), 'tp', split_axis=2, con...]
  transfers between devices with their start and end apart: 7 -> 6, of which waited for: 5 -> 4; matrix products, arithmetic and copies ran while one was open for 21% -> 17% of each run, Pallas kernels for 0% -> 0%
where the time goes in v1:
time: 266 us; the launch traced here: 265 us
  blocking collectives  120 us (45%)
  waiting for transfers between devices  44.1 us (17%)
  local copies, waits for them, and re-layouts  32.4 us (12%)
  matrix products  26.4 us (10%)
  other arithmetic  17.4 us (7%)
  between operations  14.8 us (6%)
  starting transfers between devices  9.61 us (4%)
    all_gather x2, blocking collectives, entering(): pieces = jax.tree.map(lambda part: lax.all_gather(part, axis), value)  52.5 us
    all_to_all x1, blocking collectives, local(): lax.all_to_all(partial_value.reshape(slot_shape), 'tp', split_axis=2, con...  28.1 us
    all_to_all x1, blocking collectives, local(): lax.all_to_all(x_part, 'sp', split_axis=1, concat_axis=1, tiled=True)  21.7 us
    all_to_all x1, blocking collectives, local(): lax.all_to_all(c_part, 'sp', split_axis=1, concat_axis=1, tiled=True)  17.3 us
    all_gather x1, waiting for transfers between devices, local(): lax.all_gather(c_part, 'tp', axis=2, tiled=True)  16.4 us
    all_to_all x1, waiting for transfers between devices, local(): lax.all_to_all(summed.astype(jnp.bfloat16), 'sp', split_axis=1, concat_ax...  13.7 us
    reduce_scatter x1, waiting for transfers between devices, local(): lax.psum_scatter(lax.dot_general(mid_grad, gated, (((0,), (0,)), ((), ())...  7.28 us
    all_gather x1, waiting for transfers between devices, local(): lax.all_gather(token_part.astype(jnp.bfloat16), 'tp').sum(axis=0)  6.58 us
  transfers between devices with their start and end apart: 6, of which 4 were waited for; matrix products, arithmetic and copies ran while one was open for 17% of the time, Pallas kernels for 0%

profile of v1, /device:TPU:0, one launch (start us, length us, event | category | flops | bytes accessed | tf_op | source)
XLA Modules:
  0.0 264.8 jit_solution(6914159957963554092)
XLA Ops:
  10.6 1.4 scatter_custom_fusion
  13.2 3.3 %gather_fusion.1 = bf16[512,2048]{1,0:T(8,128)(2,1)} fusion(bf16[129,2048]{1,0:T(8,128)(2,1)S(1)} %concatenate.49, s32[1024]{0:T(1024)S(1)} %get-tuple-element.176), kind=kCustom, calls=%fused_computation.1 | custom fusion | bytes 4196352 | tf_op jit(solution)/shard_map/gather | solution.py:105
  17.6 21.7 %all_to_all.27 = bf16[1,8,16,2048]{3,2,0,1:T(8,128)(2,1)} all-to-all(bf16[1,8,16,2048]{3,2,0,1:T(8,128)(2,1)S(1)} %constant_dynamic-slice_fusion.2), channel_id=1, replica_groups=mesh['sp'=8,'tp'=4] {'sp'}, dimensions={1} | all-to-all | bytes 1048576 | tf_op jit(solution)/shard_map/all_to_all | solution.py:112
  39.4 2.4 mul.210
  41.8 3.7 %mul.211 = f32[256,2048]{1,0:T(8,128)} reshape(f32[128,2,2048]{2,1,0:T(2,128)} %mul.210) | data formatting | bytes 4194304 | tf_op jit(solution)/shard_map/mul | solution.py:97
  45.7 2.1 multiply_convert_fusion
  47.9 3.3 %gather_fusion = bf16[512,2048]{1,0:T(8,128)(2,1)} fusion(bf16[257,2048]{1,0:T(8,128)(2,1)S(1)} %concatenate.48, s32[1024]{0:T(1024)S(1)} %get-tuple-element.177), kind=kCustom, calls=%fused_computation | custom fusion | bytes 4196352 | tf_op jit(solution)/shard_map/gather | solution.py:106
  52.2 17.3 %all_to_all.28 = bf16[1,8,16,2048]{3,2,0,1:T(8,128)(2,1)} all-to-all(bf16[1,8,16,2048]{3,2,0,1:T(8,128)(2,1)S(1)} %constant_dynamic-slice_fusion.3), channel_id=1, replica_groups=mesh['sp'=8,'tp'=4] {'sp'}, dimensions={1} | all-to-all | bytes 1048576 | tf_op jit(solution)/shard_map/all_to_all | solution.py:113
  69.7 3.0 %fusion.5 = f32[512,512]{1,0:T(8,128)S(1)} fusion(bf16[512,2048]{1,0:T(8,128)(2,1)} %bitcast.87, bf16[1,512,2048]{2,1,0:T(8,128)(2,1)S(1)} %copy-done), kind=kOutput, calls=%fused_computation.17 | convolution fusion | flops 1073741824 | bytes 5242880 | tf_op jit(solution)/shard_map/esd,efd->esf/dot_general | solution.py:38
  72.7 2.2 fusion.8
  75.0 16.4 %all-gather.7.cloned.1.call-done = bf16[1,8,64,2048]{3,2,0,1:T(8,128)(2,1)} async-done(((bf16[1,8,16,2048]{3,2,0,1:T(8,128)(2,1)}), bf16[1,8,64,2048]{3,2,0,1:T(8,128)(2,1)}) %all-gather.7.cloned.1.call-update) | async-done | bytes 2097168 | tf_op jit(solution)/shard_map/all_gather | solution.py:117
  91.4 4.0 %multiply_convert_fusion.2 = (bf16[512,512]{1,0:T(8,128)(2,1)S(1)}, bf16[512,512]{1,0:T(8,128)(2,1)S(1)}) fusion(f32[512,512]{1,0:T(8,128)S(1)} %fusion.5, f32[512,512]{1,0:T(8,128)} %fusion.8, bf16[512,2048]{1,0:T(8,128)(2,1)} %bitcast.91, bf16[1,512,2048]{2,1,0:T(8,128)(2,1)} %param.23), kind=kOutput, calls=%fused_computation.28 | convolution fusion | flops 1077149696 | bytes 7340032 | tf_op jit(solution)/shard_map/esd,efd->esf/dot_general | solution.py:43
  99.9 28.1 %all_to_all.29 = bf16[1,8,64,2048]{3,1,0,2:T(8,128)(2,1)S(1)} all-to-all(bf16[1,8,64,2048]{3,1,0,2:T(8,128)(2,1)S(1)} %copy.46), channel_id=1, replica_groups=mesh['sp'=8,'tp'=4] {'tp'}, dimensions={2} | all-to-all | bytes 4194304 | tf_op jit(solution)/shard_map/all_to_all | solution.py:126
  129.5 5.5 %all-to-all-start.3 = ((bf16[1,8,16,2048]{3,2,0,1:T(8,128)(2,1)}), bf16[1,8,16,2048]{3,2,0,1:T(8,128)(2,1)S(1)}, u32[]{:S(2)}, u32[]{:S(2)}) async-start(bf16[1,8,16,2048]{3,2,0,1:T(8,128)(2,1)} %copy.47), calls=%async_computation.3 | async-start | bytes 1048576 | tf_op jit(solution)/shard_map/all_to_all | solution.py:135
  135.5 13.7 %all-to-all-done.3 = bf16[1,8,16,2048]{3,2,0,1:T(8,128)(2,1)S(1)} async-done(((bf16[1,8,16,2048]{3,2,0,1:T(8,128)(2,1)}), bf16[1,8,16,2048]{3,2,0,1:T(8,128)(2,1)S(1)}, u32[]{:S(2)}, u32[]{:S(2)}) %all-to-all-start.3) | async-done | bytes 524320 | tf_op jit(solution)/shard_map/all_to_all | solution.py:135
  149.3 1.5 gather_fusion.2
  150.8 2.2 gather.14
  153.0 5.7 %multiply_reduce_fusion = bf16[128,2048]{1,0:T(8,128)(2,1)} fusion(f32[128,2,2048]{2,1,0:T(2,128)} %gather.14, f32[128,2]{1,0:T(8,128)S(1)} %reshape.239), kind=kLoop, calls=%fused_computation.24 | loop fusion | flops 786432 | bytes 2622464 | tf_op jit(solution)/shard_map/reduce_sum | solution.py:142
  158.8 3.7 %collective-permute-start = (f32[1,512]{1,0:T(1,128)S(1)}, f32[1,512]{1,0:T(1,128)S(1)}, u32[]{:S(2)}, u32[]{:S(2)}) collective-permute-start(f32[1,512]{1,0:T(1,128)S(1)} %slice.319), channel_id=1, source_target_pairs={{0,4},{4,8},{8,12},{12,16},{16,20},{20,24},{24,28},{1,5},{5,9},{9,... | collective-permute-start | bytes 6152 | tf_op jit(solution)/shard_map/ppermute | solution.py:26
  163.4 4.5 %fusion = bf16[1,512,2048]{2,1,0:T(8,128)(2,1)} fusion(bf16[512,512]{1,0:T(8,128)(2,1)S(1)} %copy-done.11, bf16[512,2048]{1,0:T(8,128)(2,1)} %bitcast.88), kind=kOutput, calls=%fused_computation.12 | convolution fusion | flops 1074790400 | bytes 4718592 | tf_op jit(solution)/shard_map/esf,esd->efd/dot_general | solution.py:48
  167.9 2.6 fusion.1
  170.5 2.7 %fusion.2 = bf16[1,512,2048]{2,1,0:T(8,128)(2,1)} fusion(bf16[512,2048]{1,0:T(8,128)(2,1)S(1)} %bitcast.92, f32[512,512]{1,0:T(8,128)S(1)} %copy-done.19, f32[512,512]{1,0:T(8,128)S(1)} %copy-done.18), kind=kOutput, calls=%fused_computation.14 | convolution fusion | flops 1076363264 | bytes 6291456 | tf_op jit(solution)/shard_map/esf,esd->efd/dot_general | solution.py:54
  173.2 6.6 %all-gather.11.cloned.1.call-done = bf16[512,2048]{1,0:T(8,128)(2,1)} async-done(((bf16[128,2048]{1,0:T(8,128)(2,1)}), bf16[512,2048]{1,0:T(8,128)(2,1)}) %all-gather.11.cloned.1.call-update) | async-done | bytes 2097168 | tf_op jit(solution)/shard_map/all_gather | solution.py:144
  179.8 2.0 reduce_sum.48
  181.9 2.1 convolution_convert_fusion
  184.0 2.7 %convert_multiply_fusion = (f32[128,512]{1,0:T(8,128)S(1)}, bf16[128,512]{1,0:T(8,128)(2,1)}) fusion(bf16[128,512]{1,0:T(8,128)(2,1)S(1)} %copy-done.9, f32[128,512]{1,0:T(8,128)S(1)} %copy-done.4, bf16[2048,512]{1,0:T(8,128)(2,1)} %param.20, bf16[128,2048]{1,0:T(8,128)(2,1)S(1)} %reduce_sum.48, bf16[128,2048]{1,0:T(8,128)(2,1)S(1)} %copy-done.3), kind=kOutput, calls=%fused_computation.33 | convolution fusion | flops 269746176 | bytes 3932160 | tf_op jit(solution)/shard_map/dot_general | solution.py:156
  190.3 26.4 %all-gather.1 = f32[8,1,512]{2,1,0:T(1,128)S(1)} all-gather(f32[1,1,512]{2,1,0:T(1,128)S(1)} %get-tuple-element.137), channel_id=1, replica_groups=mesh['sp'=8,'tp'=4] {'sp'}, dimensions={0}, use_global_device_ids=true | all-gather | bytes 18432 | tf_op jit(solution)/shard_map/all_gather | solution.py:9
  216.7 26.1 %all-gather.2 = f32[8,1,512]{2,1,0:T(1,128)S(1)} all-gather(f32[1,1,512]{2,1,0:T(1,128)S(1)} %get-tuple-element.136), channel_id=1, replica_groups=mesh['sp'=8,'tp'=4] {'sp'}, dimensions={0}, use_global_device_ids=true | all-gather | bytes 18432 | tf_op jit(solution)/shard_map/all_gather | solution.py:9
  244.8 1.7 rev.14
  246.6 1.7 rev.15
  249.2 7.3 %reduce-scatter.2.cloned.1.call-done = bf16[256,512]{1,0:T(8,128)(2,1)} async-done(((bf16[2048,512]{1,0:T(8,128)(2,1)}), bf16[256,512]{1,0:T(8,128)(2,1)}) %reduce-scatter.2.cloned.1.call-update) | async-done | bytes 262160 | tf_op jit(solution)/shard_map/reduce_scatter | solution.py:148
  256.5 1.8 convert_element_type.116
  (221 shorter events, 20.5 us)
Async XLA Ops:
  7.2 62.5 %copy-start = (bf16[1,512,2048]{2,1,0:T(8,128)(2,1)S(1)}, bf16[1,512,2048]{2,1,0:T(8,128)(2,1)}, u32[]{:S(2)}) copy-start(bf16[1,512,2048]{2,1,0:T(8,128)(2,1)} %param.21) | copy-start | bytes 6291460
  7.2 62.4 %all-gather.9.cloned.1.call-start = ((), (), s32[]{:S(2)}) async-start(), calls=%async_computation.6 | async-start | bytes 2621440 | tf_op jit(solution)/shard_map/all_gather | solution.py:116
  16.4 22.9 %copy-start.2 = (bf16[128,2048]{1,0:T(8,128)(2,1)S(1)}, bf16[128,2048]{1,0:T(8,128)(2,1)}, u32[]{:S(2)}) copy-start(bf16[128,2048]{1,0:T(8,128)(2,1)} %param.14) | copy-start | bytes 1572868
  39.3 52.1 %all-gather.7.cloned.1.call-start = ((), (), s32[]{:S(2)}) async-start(), calls=%async_computation.5 | async-start | bytes 2621440 | tf_op jit(solution)/shard_map/all_gather | solution.py:117
  41.7 3.7 %copy-start.13 = (f32[128,2]{0,1:T(2,128)S(1)}, f32[128,2]{0,1:T(2,128)}, u32[]{:S(2)}) copy-start(f32[128,2]{0,1:T(2,128)} %param.16) | copy-start | bytes 3076
  69.6 3.1 %copy-start.5 = (bf16[1,512,2048]{2,1,0:T(8,128)(2,1)S(1)}, bf16[1,512,2048]{2,1,0:T(8,128)(2,1)}, u32[]{:S(2)}) copy-start(bf16[1,512,2048]{2,1,0:T(8,128)(2,1)} %param.22) | copy-start | bytes 6291460
  69.6 3.0 %copy-start.14 = (bf16[1,8,64,2048]{3,2,0,1:T(8,128)(2,1)S(1)}, bf16[1,8,64,2048]{3,2,0,1:T(8,128)(2,1)}, u32[]{:S(2)}) copy-start(bf16[1,8,64,2048]{3,2,0,1:T(8,128)(2,1)} %all-gather.9.cloned.1.call-done) | copy-start | bytes 6291460
  72.7 18.7 %copy-start.17 = (f32[512,512]{1,0:T(8,128)}, f32[512,512]{1,0:T(8,128)S(1)}, u32[]{:S(2)}) copy-start(f32[512,512]{1,0:T(8,128)S(1)} %fusion.5) | copy-start | bytes 3145732
  95.5 1.3 copy-start.10
  95.5 1.3 copy-start.7
  95.5 2.0 copy-start.6
  129.5 19.7 %all-to-all-start.3 = ((bf16[1,8,16,2048]{3,2,0,1:T(8,128)(2,1)}), bf16[1,8,16,2048]{3,2,0,1:T(8,128)(2,1)S(1)}, u32[]{:S(2)}, u32[]{:S(2)}) async-start(bf16[1,8,16,2048]{3,2,0,1:T(8,128)(2,1)} %copy.47), calls=%async_computation.3 | async-start | bytes 1048576 | tf_op jit(solution)/shard_map/all_to_all | solution.py:135
  135.0 44.8 %all-gather.11.cloned.1.call-start = ((), (), s32[]{:S(2)}) async-start(), calls=%async_computation.8 | async-start | bytes 2621440 | tf_op jit(solution)/shard_map/all_gather | solution.py:144
  153.0 5.8 %copy-start.4 = (f32[128,512]{1,0:T(8,128)S(1)}, f32[128,512]{1,0:T(8,128)}, u32[]{:S(2)}) copy-start(f32[128,512]{1,0:T(8,128)} %param.18) | copy-start | bytes 786436
  153.0 9.5 %copy-start.12 = (f32[128,512]{1,0:T(8,128)S(1)}, f32[128,512]{1,0:T(8,128)}, u32[]{:S(2)}) copy-start(f32[128,512]{1,0:T(8,128)} %param.19) | copy-start | bytes 786436
  158.7 4.7 %copy-start.11 = (bf16[512,512]{1,0:T(8,128)(2,1)S(1)}, bf16[512,512]{1,0:T(8,128)(2,1)}, u32[]{:S(2)}) copy-start(bf16[512,512]{1,0:T(8,128)(2,1)} %copy-done.10) | copy-start | bytes 1572868
  158.8 97.7 %reduce-scatter.2.cloned.1.call-start = ((), (), s32[]{:S(2)}) async-start(), calls=%async_computation.7 | async-start | bytes 2359296 | tf_op jit(solution)/shard_map/reduce_scatter | solution.py:148
  158.8 89.5 %collective-permute-start = (f32[1,512]{1,0:T(1,128)S(1)}, f32[1,512]{1,0:T(1,128)S(1)}, u32[]{:S(2)}, u32[]{:S(2)}) collective-permute-start(f32[1,512]{1,0:T(1,128)S(1)} %slice.319), channel_id=1, source_target_pairs={{0,4},{4,8},{8,12},{12,16},{16,20},{20,24},{24,28},{1,5},{5,9},{9,... | collective-permute-start | bytes 6152 | tf_op jit(solution)/shard_map/ppermute | solution.py:26
  163.4 4.5 %copy-start.8 = (bf16[512,512]{1,0:T(8,128)(2,1)S(1)}, bf16[512,512]{1,0:T(8,128)(2,1)}, u32[]{:S(2)}) copy-start(bf16[512,512]{1,0:T(8,128)(2,1)} %copy-done.7) | copy-start | bytes 1572868
  163.4 4.5 %copy-start.15 = (bf16[1,8,64,2048]{3,2,0,1:T(8,128)(2,1)S(1)}, bf16[1,8,64,2048]{3,2,0,1:T(8,128)(2,1)}, u32[]{:S(2)}) copy-start(bf16[1,8,64,2048]{3,2,0,1:T(8,128)(2,1)} %all-gather.9.cloned.1.call-done) | copy-start | bytes 6291460
  167.9 2.6 copy-start.16
  167.9 2.6 copy-start.18
  167.9 2.6 copy-start.19
  173.2 8.6 %copy-start.3 = (bf16[128,2048]{1,0:T(8,128)(2,1)S(1)}, bf16[128,2048]{1,0:T(8,128)(2,1)}, u32[]{:S(2)}) copy-start(bf16[128,2048]{1,0:T(8,128)(2,1)} %param.14) | copy-start | bytes 1572868
  173.2 8.6 %copy-start.9 = (bf16[128,512]{1,0:T(8,128)(2,1)S(1)}, bf16[128,512]{1,0:T(8,128)(2,1)}, u32[]{:S(2)}) copy-start(bf16[128,512]{1,0:T(8,128)(2,1)} %param.17) | copy-start | bytes 393220
  243.4 14.9 %copy-start.1 = (bf16[1,512,2048]{2,1,0:T(8,128)(2,1)S(1)}, bf16[1,512,2048]{2,1,0:T(8,128)(2,1)}, u32[]{:S(2)}) copy-start(bf16[1,512,2048]{2,1,0:T(8,128)(2,1)} %param.21) | copy-start | bytes 6291460
Sparse Core Ops, SparseCore 0:
  39.4 21.5 all-gather.8
  69.7 21.6 all-gather.6
  158.9 20.8 all-gather.10
  188.1 68.3 reduce-scatter.1
